TPU v7x, 32 devices: a whole 2x2x4 slice. The times are simulated.
32 devices in a mesh: sp: 8 (over z, x), tp: 4 (over y, core).
Axes of the slice: x: 2, y: 2, z: 4, core: 2. Of those that a mesh axis runs over, the one named last changes fastest.
Arguments:
- residual: bfloat16 [4096, 2048], P('sp'), may hold values from -6 to 6
- queries: bfloat16 [4096, 1024], P('sp', 'tp'), may hold values from -384 to 384
- key_pairs: bfloat16 [4096, 1024], P('sp', 'tp'), may hold values from -384 to 384
- values: bfloat16 [4096, 1024], P('sp', 'tp'), may hold values from -6 to 6
- lambdas: float32 [8], P('tp'), may hold values from 0.3 to 0.8
- head_gain: float32 [128], replicated, may hold values from 0.1 to 1.9
- w_out: bfloat16 [1024, 2048], replicated, may hold values from -0.1875 to 0.1875
- norm_gain: float32 [2048], replicated, may hold values from 0.1 to 1.9
- w_gate: bfloat16 [2048, 5632], P('sp', 'tp'), may hold values from -0.125 to 0.125
- w_up: bfloat16 [2048, 5632], P('sp', 'tp'), may hold values from -0.125 to 0.125
- w_down: bfloat16 [5632, 2048], P('tp', 'sp'), may hold values from -0.078125 to 0.078125
Outputs:
- layer_out: bfloat16 [4096, 2048], P(('sp', 'tp'))
All inputs are finite; a program needn't handle non-finite values.
Results may differ from a plain program's by a relative error of at most 0.018.
Values may be sent and summed in bfloat16 or wider, within the bound.
A program may use at most 128 MiB of HBM per device.

v0:
```python
import functools

import jax
import jax.numpy as jnp
import numpy as np
from jax import lax
from jax.experimental import pallas as pl
from jax.experimental.pallas import tpu as pltpu
from jax.sharding import Mesh, PartitionSpec as P

HD = 64


def attend_chunk(q, k, v, m_ref, l_ref, acc_ref, slot, rows):
    scores = lax.dot_general(
        q, k, (((1,), (1,)), ((), ())), preferred_element_type=jnp.float32
    )
    old = m_ref[slot, rows, :]
    high = jnp.maximum(old, jnp.max(scores, axis=1, keepdims=True))
    shrink = jnp.exp(old - high)
    weights = jnp.exp(scores - high[:, :1])
    l_ref[slot, rows, :] = l_ref[slot, rows, :] * shrink + jnp.sum(weights, axis=1, keepdims=True)
    m_ref[slot, rows, :] = high
    acc_ref[slot, rows, :] = acc_ref[slot, rows, :] * shrink + jnp.dot(
        weights.astype(jnp.bfloat16), v, preferred_element_type=jnp.float32
    )


def finish_heads(heads, width, lam_ref, gain_ref, l_ref, acc_ref, out_ref):
    for h in range(heads):
        first = acc_ref[2 * h] / l_ref[2 * h]
        second = acc_ref[2 * h + 1] / l_ref[2 * h + 1]
        differ = first - lam_ref[h] * second
        scale = lax.rsqrt(jnp.mean(differ * differ, axis=1, keepdims=True) + 1e-05)
        out_ref[:, h * width : (h + 1) * width] = (differ * scale * gain_ref[...]).astype(out_ref.dtype)


def nearest(k, me, n):
    low, high = me, n - 1 - me
    edge = jnp.minimum(low, high)
    side = jnp.where(high >= low, 1, -1)
    near = jnp.where(k % 2 == 1, 1, -1) * ((k + 1) // 2)
    off = side * jnp.where(k <= 2 * edge, near, k - edge)
    return me + off, off


def gather_attend_kernel(
    nz, nx, heads, block,
    lam_ref, q_ref, kv_ref, gain_ref, pair_ref, down_ref,
    out_ref, pair_out, down_out,
    kv_all, m_ref, l_ref, acc_ref,
    up_sem, low_sem, side_sem, kv_sem, pz_sem, dz_sem, px_sem, dx_sem, p_sem, d_sem,
):
    z, x = lax.axis_index("z"), lax.axis_index("x")
    rows_all = q_ref.shape[0]
    width = out_ref.shape[1] // heads
    keys = heads * 2 * HD
    depth = pair_ref.shape[2]

    def remote(src, dst, send, recv, zz, xx):
        return pltpu.make_async_remote_copy(
            src_ref=src, dst_ref=dst, send_sem=send, recv_sem=recv,
            device_id={"z": zz, "x": xx}, device_id_type=pl.DeviceIdType.MESH,
        )

    barrier = pltpu.get_barrier_semaphore()
    for a in range(nz):
        for b in range(nx):
            if a + b > 0:
                pl.semaphore_signal(
                    barrier, inc=1,
                    device_id={"z": lax.rem(z + a, nz), "x": lax.rem(x + b, nx)},
                    device_id_type=pl.DeviceIdType.MESH,
                )
    pl.semaphore_wait(barrier, nz * nx - 1)

    def slot(zz, xx):
        return zz * nx + xx

    def flow(src, k, zz, go):
        off = zz - z
        here = kv_all.at[slot(zz, x)]

        @pl.when(jnp.logical_and(off <= 0, z < nz - 1))
        def _():
            go(remote(src, here, up_sem.at[k], kv_sem.at[slot(zz, x)], jnp.minimum(z + 1, nz - 1), x))

        @pl.when(jnp.logical_and(off >= 0, z > 0))
        def _():
            go(remote(src, here, low_sem.at[k], kv_sem.at[slot(zz, x)], jnp.maximum(z - 1, 0), x))

        for e in range(1, nx):
            go(remote(src, here, side_sem.at[e - 1, k], kv_sem.at[slot(zz, x)], z, lax.rem(x + e, nx)))

    def pair_place(s):
        return pair_out.at[:, pl.ds(pl.multiple_of(s * depth, depth), depth), :]

    def along(d, go):
        to = lax.rem(z + d, nz)
        s = slot(z, x)
        go(remote(pair_ref.at[to], pair_place(s), pz_sem.at[d], p_sem.at[s], to, x))
        go(remote(down_ref.at[to], down_out.at[s], dz_sem.at[d], d_sem.at[s], to, x))

    def across(src_pair, src_down, d, s, go):
        for e in range(1, nx):
            to = lax.rem(x + e, nx)
            go(remote(src_pair, pair_place(s), px_sem.at[e - 1, d], p_sem.at[s], z, to))
            go(remote(src_down, down_out.at[s], dx_sem.at[e - 1, d], d_sem.at[s], z, to))

    def arrived(src_pair, src_down, s):
        remote(src_pair, pair_place(s), pz_sem.at[0], p_sem.at[s], z, x).wait_recv()
        remote(src_down, down_out.at[s], dz_sem.at[0], d_sem.at[s], z, x).wait_recv()

    start = lambda copy: copy.start()
    sent = lambda copy: copy.wait_send()

    flow(kv_ref, 0, z, start)
    mine = slot(z, x)
    pair_out[:, pl.ds(pl.multiple_of(mine * depth, depth), depth), :] = pair_ref[z]
    down_out[mine] = down_ref[z]
    kv_all[mine] = kv_ref[...]
    m_ref[...] = jnp.full_like(m_ref, -jnp.inf)
    l_ref[...] = jnp.zeros_like(l_ref)
    acc_ref[...] = jnp.zeros_like(acc_ref)

    def attend(s):
        for h in range(heads):
            v = kv_all[s, :, keys + h * width : keys + (h + 1) * width]
            for m in range(2):
                lane = (2 * h + m) * HD
                k = kv_all[s, :, lane : lane + HD]
                for r in range(0, rows_all, block):
                    rows = pl.ds(r, block)
                    q = q_ref[rows, lane : lane + HD] * jnp.bfloat16(HD**-0.5)
                    attend_chunk(q, k, v, m_ref, l_ref, acc_ref, 2 * h + m, rows)

    def step(k, _):
        zz, _off = nearest(k, z, nz)
        here = kv_all.at[slot(zz, x)]

        @pl.when(k > 0)
        def _():
            remote(kv_ref, here, up_sem.at[k], kv_sem.at[slot(zz, x)], z, x).wait_recv()
            flow(here, k, zz, start)

        @pl.when(k == min(1, nz - 1))
        def _():
            for d in range(1, nz):
                along(d, start)
            across(pair_ref.at[z], down_ref.at[z], 0, mine, start)

        def column(e, _):
            other = lax.rem(x - e + nx, nx)

            @pl.when(e > 0)
            def _():
                remote(kv_ref, here, up_sem.at[k], kv_sem.at[slot(zz, other)], z, x).wait_recv()

            attend(slot(zz, other))
            return 0

        lax.fori_loop(0, nx, column, 0)
        return 0

    lax.fori_loop(0, nz, step, 0)
    for d in range(1, nz):
        zz = lax.rem(z - d + nz, nz)
        s = slot(zz, x)
        arrived(pair_ref.at[z], down_ref.at[z], s)
        across(pair_place(s), down_out.at[s], d, s, start)
    finish_heads(heads, width, lam_ref, gain_ref, l_ref, acc_ref, out_ref)
    for d in range(nz):
        zz = lax.rem(z - d + nz, nz)
        for e in range(1, nx):
            arrived(pair_ref.at[z], down_ref.at[z], slot(zz, lax.rem(x - e + nx, nx)))
    for d in range(nz):
        zz = lax.rem(z - d + nz, nz)
        s = slot(zz, x)
        across(pair_place(s), down_out.at[s], d, s, sent)
        if d:
            along(d, sent)

    def settle(k, _):
        zz, _off = nearest(k, z, nz)
        flow(kv_ref, k, zz, sent)
        return 0

    lax.fori_loop(0, nz, settle, 0)


def gather_attend(nz, nx, queries, kv, lambdas, head_gain, pairs, downs):
    rows = queries.shape[0]
    heads = lambdas.shape[0]
    width = head_gain.shape[0]
    _, _, depth, mine = pairs.shape
    blocks = nz * nx
    vmem = pl.BlockSpec(memory_space=pltpu.VMEM)
    dma = pltpu.SemaphoreType.DMA
    side = max(nx - 1, 1)
    return pl.pallas_call(
        functools.partial(gather_attend_kernel, nz, nx, heads, 256),
        out_shape=[
            jax.ShapeDtypeStruct((rows, heads * width), jnp.bfloat16),
            jax.ShapeDtypeStruct((2, blocks * depth, mine), jnp.bfloat16),
            jax.ShapeDtypeStruct((blocks,) + downs.shape[1:], jnp.bfloat16),
        ],
        in_specs=[pl.BlockSpec(memory_space=pltpu.SMEM)] + [vmem] * 5,
        out_specs=[vmem] * 3,
        scratch_shapes=[pltpu.VMEM((blocks,) + kv.shape, jnp.bfloat16)]
        + [pltpu.VMEM((2 * heads, rows, width), jnp.float32)] * 3
        + [
            dma((nz,)), dma((nz,)), dma((side, nz)), dma((blocks,)),
            dma((nz,)), dma((nz,)), dma((side, nz)), dma((side, nz)), dma((blocks,)), dma((blocks,)),
        ],
        compiler_params=pltpu.CompilerParams(
            collective_id=0, has_side_effects=True, vmem_limit_bytes=60 * 1024 * 1024
        ),
        cost_estimate=pl.CostEstimate(
            flops=rows * rows * blocks * heads * 4096, bytes_accessed=4000000, transcendentals=0
        ),
        name="gather_attend",
    )(lambdas, queries, kv, head_gain.reshape(1, width), pairs, downs)


def per_device(
    nz, nx, residual, queries, key_pairs, values, lambdas, head_gain, w_out, norm_gain, w_gate, w_up, w_down
):
    local_rows = queries.shape[0]
    heads_here = lambdas.shape[0]
    value_width = head_gain.shape[0]
    d_rows, units = w_gate.shape
    mine = units // nz
    width = residual.shape[1]

    kv = jnp.concatenate([key_pairs, values], axis=1)
    pairs = jnp.stack([w_gate.reshape(d_rows, nz, mine), w_up.reshape(d_rows, nz, mine)], axis=2)
    pairs = jnp.transpose(pairs, (1, 2, 0, 3))
    heads_out, both, downs = gather_attend(
        nz, nx, queries, kv, lambdas, head_gain, pairs, w_down.reshape(nz, mine, w_down.shape[1])
    )
    gate, up = both[0], both[1]
    down = jnp.transpose(downs, (1, 0, 2)).reshape(mine, width)
    tp_index = lax.axis_index("tp")
    own_rows = local_rows // lax.axis_size("tp")
    w_mine = lax.dynamic_slice_in_dim(
        w_out, tp_index * heads_here * value_width, heads_here * value_width, 0
    )
    projected = lax.psum_scatter(
        jnp.dot(heads_out, w_mine, preferred_element_type=jnp.float32).astype(jnp.bfloat16),
        "tp",
        scatter_dimension=0,
        tiled=True,
    ).astype(jnp.float32)
    residual_own = lax.dynamic_slice_in_dim(residual, tp_index * own_rows, own_rows, 0)
    hidden_own = (residual_own.astype(jnp.float32) + projected).astype(jnp.bfloat16)
    stream_f = hidden_own.astype(jnp.float32)
    scaled = stream_f * lax.rsqrt(jnp.mean(stream_f * stream_f, axis=-1, keepdims=True) + 1e-05)
    normed_rows = lax.all_gather(
        (scaled * norm_gain).astype(jnp.bfloat16), ("z", "tp"), axis=0, tiled=True
    )
    gate_sum = jnp.dot(normed_rows, gate, preferred_element_type=jnp.float32)
    up_sum = jnp.dot(normed_rows, up, preferred_element_type=jnp.float32)
    hidden_units = (jax.nn.silu(gate_sum) * up_sum).astype(jnp.bfloat16)
    ffn_out = lax.psum_scatter(
        jnp.dot(hidden_units, down, preferred_element_type=jnp.float32).astype(jnp.bfloat16),
        ("z", "tp"),
        scatter_dimension=0,
        tiled=True,
    ).astype(jnp.float32)
    return (hidden_own.astype(jnp.float32) + ffn_out).astype(jnp.bfloat16)


def solution(mesh):
    sp, tp = mesh.shape["sp"], mesh.shape["tp"]
    coords = [getattr(d, "coords", None) for d in mesh.devices.flat]
    nx = len({c[0] for c in coords}) if all(c is not None for c in coords) else 2
    if sp % nx:
        nx = 1
    nz = sp // nx
    cube = Mesh(np.asarray(mesh.devices).reshape(nz, nx, tp), ("z", "x", "tp"))
    zx = ("z", "x")
    placed = (
        P(zx, None),
        P(zx, "tp"),
        P(zx, "tp"),
        P(zx, "tp"),
        P("tp"),
        P(),
        P(),
        P(),
        P(zx, "tp"),
        P(zx, "tp"),
        P("tp", zx),
    )
    return jax.shard_map(
        functools.partial(per_device, nz, nx),
        mesh=cube,
        in_specs=placed,
        out_specs=P(("z", "x", "tp"), None),
        check_vma=False,
    )
```

profile of v0, /device:TPU:0, one launch (start us, length us, event | category | flops | bytes accessed | tf_op | source)
XLA Modules:
  0.0 403.6 jit_solution(15631480809438367702)
XLA Ops:
  6.5 0.0 copy-start.1
  6.5 0.0 reduce-scatter.3.cloned.1.call-start
  6.5 0.0 copy-start.2
  6.5 0.0 copy-start.3
  6.5 1.5 copy.12
  8.0 0.4 copy.14
  8.4 0.0 copy-done.1
  8.4 0.3 copy.13
  8.7 0.4 copy.15
  9.0 0.0 copy-done.2
  9.1 0.0 copy-done.3
  9.1 0.8 pad_maximum_fusion.kv_ref
  9.9 1.4 maximum_bitcast_fusion.pair_ref
  11.3 153.6 %gather_attend.1 = (bf16[512,256]{1,0:T(8,128)(2,1)}, bf16[2,2048,352]{2,1,0:T(8,128)(2,1)}, bf16[8,352,256]{2,1,0:T(8,128)(2,1)}) custom-call(f32[2]{0:T(128)} %lam_ref.1, bf16[512,256]{1,0:T(8,128)(2,1)} %q_ref.1, bf16[512,512]{1,0:T(8,128)(2,1)} %pad_maximum_fusion.kv_ref, f32[1,128]{1,0:T(1,128)} %bitcast.25, ...), custom_call_target="tpu_custom_call" | custom-call | flops 17179869184 | bytes 4000000 | tf_op jit(solution)/shard_map/gather_attend/pallas_call | solution.py:200
  164.9 3.4 convolution_convert_fusion.1
  168.3 0.0 copy-start.4
  168.3 0.0 copy-start
  168.3 0.0 reduce-scatter.3.cloned.1.call-update
  168.3 0.0 all-gather.2.cloned.1.call-start
  168.4 29.5 %reduce-scatter.3.cloned.1.call-done = bf16[128,2048]{1,0:T(8,128)(2,1)} async-done(((bf16[512,2048]{1,0:T(8,128)(2,1)}), bf16[128,2048]{1,0:T(8,128)(2,1)}) %reduce-scatter.3.cloned.1.call-update) | async-done | bytes 524304 | tf_op jit(solution)/shard_map/reduce_scatter | solution.py:248
  197.9 1.5 fusion.6
  199.3 0.0 copy-done.4
  199.3 1.0 fusion.8
  200.3 0.0 all-gather.2.cloned.1.call-update
  200.4 0.2 reduce-scatter.5.cloned.1.call-start
  200.6 0.0 copy-done
  200.6 0.2 copy.17
  200.8 74.0 %all-gather.2.cloned.1.call-done = bf16[2048,2048]{1,0:T(8,128)(2,1)} async-done(((bf16[128,2048]{1,0:T(8,128)(2,1)}), bf16[2048,2048]{1,0:T(8,128)(2,1)}) %all-gather.2.cloned.1.call-update) | async-done | bytes 8388624 | tf_op jit(solution)/shard_map/all_gather | solution.py:258
  274.8 0.0 copy-start.5
  274.8 0.0 copy-start.6
  274.8 6.4 %fusion.2 = f32[2048,352]{0,1:T(8,128)S(1)} fusion(bf16[2048,2048]{1,0:T(8,128)(2,1)} %all-gather.2.cloned.1.call-done, bf16[2,2048,352]{2,1,0:T(8,128)(2,1)} %get-tuple-element.9), kind=kOutput, calls=%fused_computation.6 | convolution fusion | flops 2952790016 | bytes 12845056 | tf_op jit(solution)/shard_map/dot_general | solution.py:261
  281.2 0.0 copy-done.5
  281.2 0.7 copy-done.6
  282.0 4.0 fusion
  286.0 6.9 %convolution_convert_fusion = bf16[2048,2048]{1,0:T(8,128)(2,1)} fusion(bf16[2048,352]{0,1:T(8,128)(2,1)S(1)} %fusion, bf16[352,2048]{1,0:T(8,128)(2,1)S(1)} %bitcast.23), kind=kOutput, calls=%fused_computation | convolution fusion | flops 2956984320 | bytes 11272192 | tf_op jit(solution)/shard_map/dot_general | solution.py:265
  292.9 0.0 reduce-scatter.5.cloned.1.call-update
  292.9 102.2 %reduce-scatter.5.cloned.1.call-done = bf16[128,2048]{1,0:T(8,128)(2,1)} async-done(((bf16[2048,2048]{1,0:T(8,128)(2,1)}), bf16[128,2048]{1,0:T(8,128)(2,1)}) %reduce-scatter.5.cloned.1.call-update) | async-done | bytes 524304 | tf_op jit(solution)/shard_map/reduce_scatter | solution.py:264
  395.1 2.0 fusion.9
  (1 shorter events, 0.0 us)
Async XLA Ops:
  6.5 1.9 copy-start.1
  6.5 191.3 %reduce-scatter.3.cloned.1.call-start = ((), (), s32[]{:S(2)}) async-start(), calls=%async_computation.2 | async-start | bytes 2621440 | tf_op jit(solution)/shard_map/reduce_scatter | solution.py:248
  6.5 2.5 copy-start.2
  6.5 2.5 copy-start.3
  168.3 31.1 %copy-start.4 = (f32[2048]{0:T(1024)S(1)}, f32[2048]{0:T(1024)}, u32[]{:S(2)}) copy-start(f32[2048]{0:T(1024)} %param.18) | copy-start | bytes 24580
  168.3 32.3 %copy-start = (bf16[8,352,256]{2,1,0:T(8,128)(2,1)S(1)}, bf16[8,352,256]{2,1,0:T(8,128)(2,1)}, u32[]{:S(2)}) copy-start(bf16[8,352,256]{2,1,0:T(8,128)(2,1)} %get-tuple-element.10) | copy-start | bytes 4325380
  168.3 106.5 %all-gather.2.cloned.1.call-start = ((), (), s32[]{:S(2)}) async-start(), calls=%async_computation.3 | async-start | bytes 8912896 | tf_op jit(solution)/shard_map/all_gather | solution.py:258
  200.4 194.7 %reduce-scatter.5.cloned.1.call-start = ((), (), s32[]{:S(2)}) async-start(), calls=%async_computation.4 | async-start | bytes 8912896 | tf_op jit(solution)/shard_map/reduce_scatter | solution.py:264
  274.8 6.4 %copy-start.5 = (bf16[2048,2048]{1,0:T(8,128)(2,1)S(1)}, bf16[2048,2048]{1,0:T(8,128)(2,1)}, u32[]{:S(2)}) copy-start(bf16[2048,2048]{1,0:T(8,128)(2,1)} %all-gather.2.cloned.1.call-done) | copy-start | bytes 25165828
  274.8 7.2 %copy-start.6 = (bf16[2,2048,352]{2,1,0:T(8,128)(2,1)S(1)}, bf16[2,2048,352]{2,1,0:T(8,128)(2,1)}, u32[]{:S(2)}) copy-start(bf16[2,2048,352]{2,1,0:T(8,128)(2,1)} %get-tuple-element.9) | copy-start | bytes 8650756
Sparse Core Ops, SparseCore 0:
  168.4 29.3 reduce-scatter.2
  200.5 74.2 all-gather.1
  293.0 102.0 reduce-scatter.4
where the time goes:
time: 404 us
  waiting for transfers between devices  206 us (51%)
  Pallas kernels  154 us (38%)
  matrix products  20.7 us (5%)
  between operations  13.2 us (3%)
  other arithmetic  6.68 us (2%)
    pallas_call x1, Pallas kernels, gather_attend(): pl.pallas_call(functools.partial(gather_attend_kernel, nz, nx, heads, 256...  154 us
    reduce_scatter x1, waiting for transfers between devices, per_device(): lax.psum_scatter(jnp.dot(hidden_units, down, preferred_element_type=jnp.f...  102 us
    all_gather x1, waiting for transfers between devices, per_device(): lax.all_gather((scaled * norm_gain).astype(jnp.bfloat16), ('z', 'tp'), ax...  74 us
    reduce_scatter x1, waiting for transfers between devices, per_device(): lax.psum_scatter(jnp.dot(heads_out, w_mine, preferred_element_type=jnp.fl...  29.5 us
  transfers between devices with their start and end apart: 3, of which 3 were waited for; matrix products, arithmetic and copies ran while one was open for 0% of the time, Pallas kernels for 0%

commit v1 on v0

--- a/solution.py
+++ b/solution.py
@@ -222,6 +222,108 @@
     )(lambdas, queries, kv, head_gain.reshape(1, width), pairs, downs)
 
 
+def gather_rows_kernel(nz, nt, own_ref, out_ref, up_sem, low_sem, y_sem, c_sem, got_sem):
+    z, t = lax.axis_index("z"), lax.axis_index("tp")
+    rows = own_ref.shape[0]
+    partner = t + 1 - 2 * lax.rem(t, 2)
+
+    barrier = pltpu.get_barrier_semaphore()
+    for a in range(nz):
+        for b in range(nt):
+            if a + b > 0:
+                pl.semaphore_signal(
+                    barrier, inc=1,
+                    device_id={"z": lax.rem(z + a, nz), "tp": lax.rem(t + b, nt)},
+                    device_id_type=pl.DeviceIdType.MESH,
+                )
+    pl.semaphore_wait(barrier, nz * nt - 1)
+
+    def place(zz, tt):
+        s = zz * nt + tt
+        return out_ref.at[pl.ds(pl.multiple_of(s * rows, rows), rows), :], got_sem.at[s]
+
+    def remote(src, zz, tt, send, to_z, to_t):
+        dst, recv = place(zz, tt)
+        return pltpu.make_async_remote_copy(
+            src_ref=src, dst_ref=dst, send_sem=send, recv_sem=recv,
+            device_id={"z": to_z, "tp": to_t}, device_id_type=pl.DeviceIdType.MESH,
+        )
+
+    def flow(src, k, zz, go):
+        @pl.when(jnp.logical_and(zz <= z, z < nz - 1))
+        def _():
+            go(remote(src, zz, t, up_sem.at[k], jnp.minimum(z + 1, nz - 1), t))
+
+        @pl.when(jnp.logical_and(zz >= z, z > 0))
+        def _():
+            go(remote(src, zz, t, low_sem.at[k], jnp.maximum(z - 1, 0), t))
+
+        for e in range(1, nt // 2):
+            go(remote(src, zz, t, y_sem.at[k, e], z, lax.rem(t + 2 * e, nt)))
+        go(remote(src, zz, t, c_sem.at[k, 0], z, partner))
+
+    start = lambda copy: copy.start()
+    sent = lambda copy: copy.wait_send()
+
+    def await_block(zz, tt):
+        remote(own_ref, zz, tt, c_sem.at[0, 0], z, partner).wait_recv()
+
+    flow(own_ref, 0, z, start)
+    mine, _sem = place(z, t)
+    mine[...] = own_ref[...]
+
+    def same_core(e):
+        return lax.rem(t - 2 * e + nt, nt)
+
+    def step(k, _):
+        zz, _off = nearest(k, z, nz)
+
+        @pl.when(k > 0)
+        def _():
+            await_block(zz, t)
+            flow(place(zz, t)[0], k, zz, start)
+
+        for e in range(1, nt // 2):
+            tt = same_core(e)
+            await_block(zz, tt)
+            remote(place(zz, tt)[0], zz, tt, c_sem.at[k, e], z, partner).start()
+        return 0
+
+    lax.fori_loop(0, nz, step, 0)
+
+    def settle(k, _):
+        zz, _off = nearest(k, z, nz)
+        flow(own_ref, k, zz, sent)
+        for e in range(nt // 2):
+            await_block(zz, lax.rem(partner - 2 * e + nt, nt))
+            if e:
+                tt = same_core(e)
+                remote(own_ref, zz, tt, c_sem.at[k, e], z, partner).wait_send()
+        return 0
+
+    lax.fori_loop(0, nz, settle, 0)
+
+
+def gather_rows(nz, nt, own):
+    rows, width = own.shape
+    if nt % 2:
+        return lax.all_gather(own, ("z", "tp"), axis=0, tiled=True)
+    vmem = pl.BlockSpec(memory_space=pltpu.VMEM)
+    dma = pltpu.SemaphoreType.DMA
+    return pl.pallas_call(
+        functools.partial(gather_rows_kernel, nz, nt),
+        out_shape=jax.ShapeDtypeStruct((nz * nt * rows, width), own.dtype),
+        in_specs=[vmem],
+        out_specs=vmem,
+        scratch_shapes=[dma((nz,)), dma((nz,)), dma((nz, nt // 2)), dma((nz, nt // 2)), dma((nz * nt,))],
+        compiler_params=pltpu.CompilerParams(
+            collective_id=1, has_side_effects=True, vmem_limit_bytes=32 * 1024 * 1024
+        ),
+        cost_estimate=pl.CostEstimate(flops=10**10, bytes_accessed=4000000, transcendentals=0),
+        name="gather_rows",
+    )(own)
+
+
 def per_device(
     nz, nx, residual, queries, key_pairs, values, lambdas, head_gain, w_out, norm_gain, w_gate, w_up, w_down
 ):
@@ -255,9 +357,7 @@
     hidden_own = (residual_own.astype(jnp.float32) + projected).astype(jnp.bfloat16)
     stream_f = hidden_own.astype(jnp.float32)
     scaled = stream_f * lax.rsqrt(jnp.mean(stream_f * stream_f, axis=-1, keepdims=True) + 1e-05)
-    normed_rows = lax.all_gather(
-        (scaled * norm_gain).astype(jnp.bfloat16), ("z", "tp"), axis=0, tiled=True
-    )
+    normed_rows = gather_rows(nz, lax.axis_size("tp"), (scaled * norm_gain).astype(jnp.bfloat16))
     gate_sum = jnp.dot(normed_rows, gate, preferred_element_type=jnp.float32)
     up_sum = jnp.dot(normed_rows, up, preferred_element_type=jnp.float32)
     hidden_units = (jax.nn.silu(gate_sum) * up_sum).astype(jnp.bfloat16)

time: 404 us -> 391 us (0.968)
  waiting for transfers between devices: 206 us -> 132 us
  Pallas kernels: 154 us -> 219 us
    all_gather x1 -> x0, waiting for transfers between devices: 74 us -> none  [per_device(): lax.all_gather((scaled * norm_gain).astype(jnp.bfloat16), ('z', 'tp'), ax...]
    pallas_call x0 -> x1, Pallas kernels: none -> 65.2 us  [gather_rows(): pl.pallas_call(functools.partial(gather_rows_kernel, nz, nt), out_shape=j...]
  transfers between devices with their start and end apart: 3 -> 2, of which waited for: 3 -> 2; matrix products, arithmetic and copies ran while one was open for 0% -> 0% of each run, Pallas kernels for 0% -> 0%
where the time goes in v1:
time: 391 us
  Pallas kernels  219 us (56%)
  waiting for transfers between devices  132 us (34%)
  matrix products  17.7 us (5%)
  between operations  13.5 us (3%)
  other arithmetic  5.9 us (2%)
    pallas_call x1, Pallas kernels, gather_attend(): pl.pallas_call(functools.partial(gather_attend_kernel, nz, nx, heads, 256...  154 us
    reduce_scatter x1, waiting for transfers between devices, per_device(): lax.psum_scatter(jnp.dot(hidden_units, down, preferred_element_type=jnp.f...  103 us
    pallas_call x1, Pallas kernels, gather_rows(): pl.pallas_call(functools.partial(gather_rows_kernel, nz, nt), out_shape=j...  65.2 us
    reduce_scatter x1, waiting for transfers between devices, per_device(): lax.psum_scatter(jnp.dot(heads_out, w_mine, preferred_element_type=jnp.fl...  29.1 us
  transfers between devices with their start and end apart: 2, of which 2 were waited for; matrix products, arithmetic and copies ran while one was open for 0% of the time, Pallas kernels for 0%

profile of v1, /device:TPU:0, one launch (start us, length us, event | category | flops | bytes accessed | tf_op | source)
XLA Modules:
  0.0 390.7 jit_solution(13355501681164366716)
XLA Ops:
  6.5 0.0 copy-start.1
  6.5 0.0 reduce-scatter.3.cloned.1.call-start
  6.5 0.0 copy-start.2
  6.5 0.0 copy-start.3
  6.5 1.5 copy.12
  8.0 0.4 copy.14
  8.4 0.0 copy-done.1
  8.4 0.3 copy.13
  8.7 0.4 copy.15
  9.0 0.0 copy-done.2
  9.1 0.0 copy-done.3
  9.1 0.8 pad_maximum_fusion.kv_ref
  9.9 1.4 maximum_bitcast_fusion.pair_ref
  11.3 153.7 %gather_attend.1 = (bf16[512,256]{1,0:T(8,128)(2,1)}, bf16[2,2048,352]{2,1,0:T(8,128)(2,1)}, bf16[8,352,256]{2,1,0:T(8,128)(2,1)}) custom-call(f32[2]{0:T(128)} %lam_ref.1, bf16[512,256]{1,0:T(8,128)(2,1)} %q_ref.1, bf16[512,512]{1,0:T(8,128)(2,1)} %pad_maximum_fusion.kv_ref, f32[1,128]{1,0:T(1,128)} %bitcast.25, ...), custom_call_target="tpu_custom_call" | custom-call | flops 17179869184 | bytes 4000000 | tf_op jit(solution)/shard_map/gather_attend/pallas_call | solution.py:200
  165.0 0.0 copy-start
  165.0 3.5 convolution_convert_fusion.1
  168.5 0.0 copy-start.4
  168.5 0.0 reduce-scatter.3.cloned.1.call-update
  168.5 0.2 reduce-scatter.5.cloned.1.call-start
  168.8 0.0 copy-done
  168.8 0.2 copy.17
  168.9 29.1 %reduce-scatter.3.cloned.1.call-done = bf16[128,2048]{1,0:T(8,128)(2,1)} async-done(((bf16[512,2048]{1,0:T(8,128)(2,1)}), bf16[128,2048]{1,0:T(8,128)(2,1)}) %reduce-scatter.3.cloned.1.call-update) | async-done | bytes 524304 | tf_op jit(solution)/shard_map/reduce_scatter | solution.py:350
  198.1 1.5 fusion.6
  199.5 0.0 copy-done.4
  199.6 0.2 fusion.8.own_ref
  199.8 0.0 copy-start.5
  199.8 65.2 %gather_rows.1 = bf16[2048,2048]{1,0:T(8,128)(2,1)S(1)} custom-call(bf16[128,2048]{1,0:T(8,128)(2,1)S(1)} %fusion.8.own_ref), custom_call_target="tpu_custom_call" | custom-call | flops 10000000000 | bytes 4000000 | tf_op jit(solution)/shard_map/gather_rows/pallas_call | solution.py:313
  265.0 0.0 copy-done.5
  265.0 3.3 fusion.2
  268.3 4.0 %fusion = bf16[2048,352]{0,1:T(8,128)(2,1)S(1)} fusion(bf16[2048,2048]{1,0:T(8,128)(2,1)S(1)} %gather_rows.1, f32[2048,352]{0,1:T(8,128)S(1)} %fusion.2, bf16[2,2048,352]{2,1,0:T(8,128)(2,1)S(1)} %copy-done.5), kind=kOutput, calls=%fused_computation.3 | convolution fusion | flops 2957115392 | bytes 14286848 | tf_op jit(solution)/shard_map/dot_general | solution.py:362
  272.3 6.9 %convolution_convert_fusion = bf16[2048,2048]{1,0:T(8,128)(2,1)} fusion(bf16[2048,352]{0,1:T(8,128)(2,1)S(1)} %fusion, bf16[352,2048]{1,0:T(8,128)(2,1)S(1)} %bitcast.22), kind=kOutput, calls=%fused_computation | convolution fusion | flops 2956984320 | bytes 11272192 | tf_op jit(solution)/shard_map/dot_general | solution.py:365
  279.2 0.0 reduce-scatter.5.cloned.1.call-update
  279.3 102.7 %reduce-scatter.5.cloned.1.call-done = bf16[128,2048]{1,0:T(8,128)(2,1)} async-done(((bf16[2048,2048]{1,0:T(8,128)(2,1)}), bf16[128,2048]{1,0:T(8,128)(2,1)}) %reduce-scatter.5.cloned.1.call-update) | async-done | bytes 524304 | tf_op jit(solution)/shard_map/reduce_scatter | solution.py:364
  381.9 2.0 fusion.9
  (1 shorter events, 0.0 us)
Async XLA Ops:
  6.5 1.9 copy-start.1
  6.5 191.5 %reduce-scatter.3.cloned.1.call-start = ((), (), s32[]{:S(2)}) async-start(), calls=%async_computation.2 | async-start | bytes 2621440 | tf_op jit(solution)/shard_map/reduce_scatter | solution.py:350
  6.5 2.5 copy-start.2
  6.5 2.5 copy-start.3
  165.0 3.7 copy-start
  168.5 31.0 %copy-start.4 = (f32[2048]{0:T(1024)S(1)}, f32[2048]{0:T(1024)}, u32[]{:S(2)}) copy-start(f32[2048]{0:T(1024)} %param.18) | copy-start | bytes 24580
  168.5 213.4 %reduce-scatter.5.cloned.1.call-start = ((), (), s32[]{:S(2)}) async-start(), calls=%async_computation.3 | async-start | bytes 8912896 | tf_op jit(solution)/shard_map/reduce_scatter | solution.py:364
  199.8 65.3 %copy-start.5 = (bf16[2,2048,352]{2,1,0:T(8,128)(2,1)S(1)}, bf16[2,2048,352]{2,1,0:T(8,128)(2,1)}, u32[]{:S(2)}) copy-start(bf16[2,2048,352]{2,1,0:T(8,128)(2,1)} %get-tuple-element.9) | copy-start | bytes 8650756
Sparse Core Ops, SparseCore 0:
  168.6 29.3 reduce-scatter.2
  279.4 102.5 reduce-scatter.4
